TPU v7x, 32 devices: a whole 2x2x4 slice. The times are simulated.
32 devices in a mesh: fs: 4 (over y, x), tp: 8 (over z, core).
Axes of the slice: x: 2, y: 2, z: 4, core: 2. Of those that a mesh axis runs over, the one named last changes fastest.
Arguments:
- saved_inputs: bfloat16 [2688, 4096], P('fs', 'tp'), may hold values from -6 to 6
- proj_cotangent: bfloat16 [2688, 4096], P('fs', 'tp'), may hold values from -0.115722656 to 0.115722656
- saved_hidden: bfloat16 [2688, 4096], P('fs', 'tp'), may hold values from -6 to 6
- out_cotangent: bfloat16 [2688, 4096], P('fs', 'tp'), may hold values from -0.115722656 to 0.115722656
- factors: bfloat16 [2, 4096, 128], replicated, may hold values from -0.46875 to 0.46875
- w_proj: float32 [4096, 4096], P('fs', 'tp'), may hold values from -0.09375 to 0.09375
- w_out: float32 [4096, 4096], P('tp', 'fs'), may hold values from -0.09375 to 0.09375
- moment_first: float32 [2, 128, 4096], P(None, None, 'tp'), may hold values from -1.8 to 1.8
- moment_second: float32 [2, 128, 4096], P(None, None, 'tp'), may hold values from 0.05 to 1
Outputs:
- proj_next: float32 [4096, 4096], P('fs', 'tp')
- out_next: float32 [4096, 4096], P('tp', 'fs')
- proj_copy: bfloat16 [4096, 4096], P(None, 'tp')
- out_copy: bfloat16 [4096, 4096], P('tp')
- first_next: float32 [2, 128, 4096], P(None, None, 'tp')
- second_next: float32 [2, 128, 4096], P(None, None, 'tp')
All inputs are finite; a program needn't handle non-finite values.
Results may differ from a plain program's by a relative error of at most 0.001.
Values may be sent and summed in bfloat16 or wider, within the bound.
A program may use at most 64 MiB of HBM per device.

v0:
```python
import jax
import jax.numpy as jnp
from jax import lax
from jax.sharding import PartitionSpec as P

beta_first = 0.9
beta_second = 0.95
learn_rate = 0.02
epsilon = 1e-06


def over_tokens(left_rows, right_rows, precise):
    return lax.dot_general(
        left_rows,
        right_rows,
        (((0,), (0,)), ((), ())),
        preferred_element_type=jnp.float32,
        precision=precise,
    )


def body(
    saved_inputs,
    proj_cotangent,
    saved_hidden,
    out_cotangent,
    factors,
    w_proj,
    w_out,
    moment_first,
    moment_second,
):
    highest = lax.Precision.HIGHEST
    fs_count = lax.axis_size("fs")
    tp_count = lax.axis_size("tp")
    d_model = factors.shape[1]
    hidden_width = proj_cotangent.shape[1]
    fs_rows = d_model // fs_count
    tp_feats = saved_inputs.shape[1]
    own_rows = lax.dynamic_slice_in_dim(factors, lax.axis_index("fs") * fs_rows, fs_rows, 1).astype(
        jnp.float32
    )
    own_feats = lax.dynamic_slice_in_dim(factors, lax.axis_index("tp") * tp_feats, tp_feats, 1)
    proj_rows = jnp.dot(saved_inputs, own_feats[0], preferred_element_type=jnp.float32)
    out_rows = jnp.dot(out_cotangent, own_feats[1], preferred_element_type=jnp.float32)
    proj_rows, out_rows = lax.psum((proj_rows, out_rows), "tp")
    partial_sums = jnp.stack(
        [
            over_tokens(proj_rows, proj_cotangent.astype(jnp.float32), highest),
            over_tokens(out_rows, saved_hidden.astype(jnp.float32), highest),
        ]
    )
    small_grads = lax.psum(partial_sums, "fs")
    first_next = beta_first * moment_first + (1.0 - beta_first) * small_grads
    second_next = beta_second * moment_second + (1.0 - beta_second) * small_grads * small_grads
    direction = first_next / (jnp.sqrt(second_next) + epsilon)
    update_full = jnp.einsum("kdr,kre->kde", own_rows, direction, precision=highest)
    squares = lax.psum(jnp.sum(update_full * update_full, axis=(1, 2)), ("fs", "tp"))
    norm_scale = lax.rsqrt(squares / (d_model * hidden_width * tp_count) + epsilon)
    stepped = update_full * norm_scale[:, None, None]
    proj_next = w_proj - learn_rate * stepped[0]
    out_next = w_out - learn_rate * stepped[1].T
    proj_copy, out_copy = (
        lax.all_gather(proj_next.astype(jnp.bfloat16), "fs", axis=0, tiled=True),
        lax.all_gather(out_next.astype(jnp.bfloat16), "fs", axis=1, tiled=True),
    )
    return (proj_next, out_next, proj_copy, out_copy, first_next, second_next)


def solution(mesh):
    placed = (
        P("fs", "tp"),
        P("fs", "tp"),
        P("fs", "tp"),
        P("fs", "tp"),
        P(),
        P("fs", "tp"),
        P("tp", "fs"),
        P(None, None, "tp"),
        P(None, None, "tp"),
    )
    return jax.shard_map(
        body,
        mesh=mesh,
        in_specs=placed,
        out_specs=(
            P("fs", "tp"),
            P("tp", "fs"),
            P(None, "tp"),
            P("tp", None),
            P(None, None, "tp"),
            P(None, None, "tp"),
        ),
        check_vma=False,
    )
```

profile of v0, /device:TPU:0, one launch (start us, length us, event | category | flops | bytes accessed | tf_op | source)
XLA Modules:
  0.0 292.3 jit_solution(14841451723777137700)
XLA Ops:
  7.2 1.5 copy-done
  8.8 2.3 convolution_bitcast_fusion.1
  11.1 2.2 convolution_bitcast_fusion
  13.3 0.0 all-reduce.4.cloned.1.call-start
  13.3 60.8 %all-reduce.6.cloned.1.call-done = (f32[672,128]{0,1:T(8,128)}, f32[672,128]{0,1:T(8,128)}) async-done(((f32[672,128]{0,1:T(8,128)}, f32[672,128]{0,1:T(8,128)}), (f32[672,128]{0,1:T(8,128)}, f32[672,128]{0,1:T(8,128)})) %all-reduce.6.cloned.1.call-update) | async-done | bytes 688144 | tf_op jit(solution)/shard_map/psum | solution.py:46
  74.1 1.5 convolution_bitcast_fusion.2
  75.6 1.5 convolution_bitcast_fusion.3
  77.1 0.8 pad_maximum_fusion
  77.9 0.0 all-gather.5.cloned.1.call-start
  78.0 2.9 copy.15
  80.9 41.7 %all-reduce.4.cloned.1.call-done = f32[2,128,512]{2,1,0:T(8,128)} async-done(((f32[2,128,512]{2,1,0:T(8,128)}), f32[2,128,512]{2,1,0:T(8,128)}) %all-reduce.4.cloned.1.call-update) | async-done | bytes 524304 | tf_op jit(solution)/shard_map/psum | solution.py:53
  122.6 1.6 fusion.4
  124.2 4.0 %multiply_reduce_fusion = (f32[2]{0:T(128)S(1)}, f32[2,1024,512]{2,1,0:T(8,128)}) fusion(f32[2,128,512]{2,1,0:T(8,128)S(1)} %get-tuple-element.32, f32[2,128,512]{2,1,0:T(8,128)S(1)} %get-tuple-element.33, bf16[2,4096,128]{2,1,0:T(8,128)(2,1)S(1)} %copy-done, s32[]{:T(128)S(6)} %select_n.6), kind=kOutput, calls=%fused_computation | convolution fusion | flops 1612972032 | bytes 5767180 | tf_op jit(solution)/shard_map/kdr,kre->kde/dot_general | solution.py:57
  128.2 39.2 %psum.31 = f32[2]{0:T(128)S(1)} all-reduce(f32[2]{0:T(128)S(1)} %get-tuple-element.20), channel_id=1, replica_groups=mesh['fs'=4,'tp'=8] {'fs','tp'}, use_global_device_ids=true, to_apply=%region_4.0 | all-reduce | flops 2 | bytes 16 | tf_op jit(solution)/shard_map/psum | solution.py:58
  167.4 3.1 %broadcast_multiply_fusion = f32[2,1024,512]{2,1,0:T(8,128)S(1)} fusion(f32[2,1024,512]{2,1,0:T(8,128)} %get-tuple-element.21, f32[2]{0:T(128)S(1)} %add_rsqrt_fusion), kind=kLoop, calls=%fused_computation.7 | loop fusion | flops 1048576 | bytes 8388616 | tf_op jit(solution)/shard_map/mul | solution.py:60
  170.6 2.6 fusion.15
  173.2 0.4 copy-done.1
  173.6 0.0 all-gather.3.cloned.1.call-start
  173.6 4.5 %fusion.17 = (bf16[1024,512]{1,0:T(8,128)(2,1)}, f32[1024,512]{1,0:T(8,128)}) fusion(f32[1024,512]{1,0:T(8,128)} %param.14, f32[2,1024,512]{2,1,0:T(8,128)} %copy-done.1), kind=kLoop, calls=%fused_computation.30 | loop fusion | flops 1572864 | bytes 7340032 | tf_op jit(solution)/shard_map/convert_element_type | solution.py:64
  178.1 2.9 copy.16
  181.0 46.0 %all-gather.5.cloned.1.call-done = bf16[512,4096]{0,1:T(8,128)(2,1)} async-done(((bf16[512,1024]{0,1:T(8,128)(2,1)}), bf16[512,4096]{0,1:T(8,128)(2,1)}) %all-gather.5.cloned.1.call-update) | async-done | bytes 4194320 | tf_op jit(solution)/shard_map/all_gather | solution.py:65
  227.0 6.3 %copy.17 = bf16[512,4096]{1,0:T(8,128)(2,1)} copy(bf16[512,4096]{0,1:T(8,128)(2,1)} %all-gather.5.cloned.1.call-done) | data formatting | bytes 8388608
  233.3 48.0 %all-gather.3.cloned.1.call-done = bf16[4096,512]{1,0:T(8,128)(2,1)} async-done(((bf16[1024,512]{1,0:T(8,128)(2,1)}), bf16[4096,512]{1,0:T(8,128)(2,1)}) %all-gather.3.cloned.1.call-update) | async-done | bytes 4194320 | tf_op jit(solution)/shard_map/all_gather | solution.py:64
  281.3 4.5 %copy.22 = bf16[4096,512]{1,0:T(8,128)(2,1)} copy(bf16[4096,512]{1,0:T(8,128)(2,1)} %all-gather.3.cloned.1.call-done) | data formatting | bytes 8388608
  (18 shorter events, 0.1 us)
Async XLA Ops:
  7.2 1.6 copy-start
  7.2 66.9 %copy-start.5 = (bf16[672,512]{1,0:T(8,128)(2,1)S(1)}, bf16[672,512]{1,0:T(8,128)(2,1)}, u32[]{:S(2)}) copy-start(bf16[672,512]{1,0:T(8,128)(2,1)} %param.11) | copy-start | bytes 2064388
  7.2 66.9 %all-reduce.6.cloned.1.call-start = ((), (), s32[]{:S(2)}) async-start(), calls=%async_computation.3 | async-start | bytes 1572864 | tf_op jit(solution)/shard_map/psum | solution.py:46
  8.8 66.8 %copy-start.6 = (bf16[672,512]{1,0:T(8,128)(2,1)S(1)}, bf16[672,512]{1,0:T(8,128)(2,1)}, u32[]{:S(2)}) copy-start(bf16[672,512]{1,0:T(8,128)(2,1)} %param.10) | copy-start | bytes 2064388
  13.3 109.3 %all-reduce.4.cloned.1.call-start = ((), (), s32[]{:S(2)}) async-start(), calls=%async_computation | async-start | bytes 1048576 | tf_op jit(solution)/shard_map/psum | solution.py:53
  77.9 149.1 %all-gather.5.cloned.1.call-start = ((), (), s32[]{:S(2)}) async-start(), calls=%async_computation.2 | async-start | bytes 5242880 | tf_op jit(solution)/shard_map/all_gather | solution.py:65
  124.2 4.0 %copy-start.3 = (f32[2,128,512]{2,1,0:T(8,128)}, f32[2,128,512]{2,1,0:T(8,128)S(1)}, u32[]{:S(2)}) copy-start(f32[2,128,512]{2,1,0:T(8,128)S(1)} %get-tuple-element.33) | copy-start | bytes 1572868
  124.2 4.0 %copy-start.4 = (f32[2,128,512]{2,1,0:T(8,128)}, f32[2,128,512]{2,1,0:T(8,128)S(1)}, u32[]{:S(2)}) copy-start(f32[2,128,512]{2,1,0:T(8,128)S(1)} %get-tuple-element.32) | copy-start | bytes 1572868
  167.4 3.1 %copy-start.2 = (f32[512,1024]{0,1:T(8,128)S(1)}, f32[512,1024]{0,1:T(8,128)}, u32[]{:S(2)}) copy-start(f32[512,1024]{0,1:T(8,128)} %copy.15) | copy-start | bytes 6291460
  170.6 3.0 %copy-start.1 = (f32[2,1024,512]{2,1,0:T(8,128)}, f32[2,1024,512]{2,1,0:T(8,128)S(1)}, u32[]{:S(2)}) copy-start(f32[2,1024,512]{2,1,0:T(8,128)S(1)} %broadcast_multiply_fusion) | copy-start | bytes 12582916
  173.6 107.8 %all-gather.3.cloned.1.call-start = ((), (), s32[]{:S(2)}) async-start(), calls=%async_computation.1 | async-start | bytes 5242880 | tf_op jit(solution)/shard_map/all_gather | solution.py:64
Sparse Core Ops, SparseCore 0:
  13.4 60.6 all-reduce.5
  78.1 44.4 all-reduce.3
  173.7 53.2 all-gather.4
  228.7 52.5 all-gather.2
where the time goes:
time: 293 us; the launch traced here: 292 us
  waiting for transfers between devices  197 us (67%)
  blocking collectives  39.2 us (13%)
  local copies, waits for them, and re-layouts  18.5 us (6%)
  between operations  13.9 us (5%)
  other arithmetic  12.6 us (4%)
  matrix products  11.4 us (4%)
    psum x1, waiting for transfers between devices, body(): proj_rows, out_rows = lax.psum((proj_rows, out_rows), 'tp')  60.8 us
    all_gather x1, waiting for transfers between devices, body(): lax.all_gather(proj_next.astype(jnp.bfloat16), 'fs', axis=0, tiled=True)  48 us
    all_gather x1, waiting for transfers between devices, body(): lax.all_gather(out_next.astype(jnp.bfloat16), 'fs', axis=1, tiled=True)  46 us
    psum x1, waiting for transfers between devices, body(): small_grads = lax.psum(partial_sums, 'fs')  41.7 us
    psum x1, blocking collectives, body(): lax.psum(jnp.sum(update_full * update_full, axis=(1, 2)), ('fs', 'tp'))  39.2 us
    unnamed x18, local copies, waits for them, and re-layouts  18.5 us
  transfers between devices with their start and end apart: 4, of which 4 were waited for; matrix products, arithmetic and copies ran while one was open for 6% of the time, Pallas kernels for 0%

commit v1 on v0

--- a/solution.py
+++ b/solution.py
@@ -55,7 +55,8 @@
     second_next = beta_second * moment_second + (1.0 - beta_second) * small_grads * small_grads
     direction = first_next / (jnp.sqrt(second_next) + epsilon)
     update_full = jnp.einsum("kdr,kre->kde", own_rows, direction, precision=highest)
-    squares = lax.psum(jnp.sum(update_full * update_full, axis=(1, 2)), ("fs", "tp"))
+    one_axis = lax.psum(jnp.sum(update_full * update_full, axis=(1, 2)), "tp")
+    squares = lax.psum(one_axis, "fs")
     norm_scale = lax.rsqrt(squares / (d_model * hidden_width * tp_count) + epsilon)
     stepped = update_full * norm_scale[:, None, None]
     proj_next = w_proj - learn_rate * stepped[0]

time: 293 us -> 278 us (0.949)
  blocking collectives: 39.2 us -> 24.7 us
    psum x1 -> x2, blocking collectives: 39.2 us -> 24.7 us  [the longest x1 15.8 us: body(): one_axis = lax.psum(jnp.sum(update_full * update_full, axis=(1, 2)), 'tp')]
    all_gather x1, waiting for transfers between devices: 46 us -> 42.3 us  [body(): lax.all_gather(out_next.astype(jnp.bfloat16), 'fs', axis=1, tiled=True)]
  transfers between devices with their start and end apart: 4 -> 4, of which waited for: 4 -> 4; matrix products, arithmetic and copies ran while one was open for 6% -> 5% of each run, Pallas kernels for 0% -> 0%
where the time goes in v1:
time: 278 us; the launch traced here: 277 us
  waiting for transfers between devices  196 us (71%)
  blocking collectives  24.7 us (9%)
  local copies, waits for them, and re-layouts  18.7 us (7%)
  between operations  13.9 us (5%)
  other arithmetic  12.6 us (5%)
  matrix products  11.4 us (4%)
    psum x1, waiting for transfers between devices, body(): proj_rows, out_rows = lax.psum((proj_rows, out_rows), 'tp')  60.8 us
    all_gather x1, waiting for transfers between devices, body(): lax.all_gather(proj_next.astype(jnp.bfloat16), 'fs', axis=0, tiled=True)  48 us
    psum x1, waiting for transfers between devices, body(): small_grads = lax.psum(partial_sums, 'fs')  44.6 us
    all_gather x1, waiting for transfers between devices, body(): lax.all_gather(out_next.astype(jnp.bfloat16), 'fs', axis=1, tiled=True)  42.3 us
    unnamed x18, local copies, waits for them, and re-layouts  18.7 us
    psum x1, blocking collectives, body(): one_axis = lax.psum(jnp.sum(update_full * update_full, axis=(1, 2)), 'tp')  15.8 us
    psum x1, blocking collectives, body(): squares = lax.psum(one_axis, 'fs')  8.89 us
  transfers between devices with their start and end apart: 4, of which 4 were waited for; matrix products, arithmetic and copies ran while one was open for 5% of the time, Pallas kernels for 0%

profile of v1, /device:TPU:0, one launch (start us, length us, event | category | flops | bytes accessed | tf_op | source)
XLA Modules:
  0.0 277.2 jit_solution(2148853521325239321)
XLA Ops:
  7.2 1.5 copy-done
  8.8 2.3 convolution_bitcast_fusion.1
  11.1 2.2 convolution_bitcast_fusion
  13.3 0.0 all-reduce.4.cloned.1.call-start
  13.3 60.8 %all-reduce.6.cloned.1.call-done = (f32[672,128]{0,1:T(8,128)}, f32[672,128]{0,1:T(8,128)}) async-done(((f32[672,128]{0,1:T(8,128)}, f32[672,128]{0,1:T(8,128)}), (f32[672,128]{0,1:T(8,128)}, f32[672,128]{0,1:T(8,128)})) %all-reduce.6.cloned.1.call-update) | async-done | bytes 688144 | tf_op jit(solution)/shard_map/psum | solution.py:46
  74.1 1.5 convolution_bitcast_fusion.2
  75.6 1.5 convolution_bitcast_fusion.3
  77.1 0.8 pad_maximum_fusion
  78.0 44.6 %all-reduce.4.cloned.1.call-done = f32[2,128,512]{2,1,0:T(8,128)} async-done(((f32[2,128,512]{2,1,0:T(8,128)}), f32[2,128,512]{2,1,0:T(8,128)}) %all-reduce.4.cloned.1.call-update) | async-done | bytes 524304 | tf_op jit(solution)/shard_map/psum | solution.py:53
  122.6 1.6 fusion.4
  124.2 4.0 %multiply_reduce_fusion = (f32[2]{0:T(128)S(1)}, f32[2,1024,512]{2,1,0:T(8,128)}) fusion(f32[2,128,512]{2,1,0:T(8,128)S(1)} %get-tuple-element.32, f32[2,128,512]{2,1,0:T(8,128)S(1)} %get-tuple-element.33, bf16[2,4096,128]{2,1,0:T(8,128)(2,1)S(1)} %copy-done, s32[]{:T(128)S(6)} %select_n.6), kind=kOutput, calls=%fused_computation | convolution fusion | flops 1612972032 | bytes 5767180 | tf_op jit(solution)/shard_map/kdr,kre->kde/dot_general | solution.py:57
  128.2 15.8 %psum.38 = f32[2]{0:T(128)S(1)} all-reduce(f32[2]{0:T(128)S(1)} %get-tuple-element.20), channel_id=1, replica_groups=mesh['fs'=4,'tp'=8] {'tp'}, use_global_device_ids=true, to_apply=%region_4.0 | all-reduce | flops 2 | bytes 16 | tf_op jit(solution)/shard_map/psum | solution.py:58
  144.0 2.9 %copy.15 = f32[512,1024]{0,1:T(8,128)} copy(f32[512,1024]{1,0:T(8,128)} %param.15) | data formatting | bytes 4194304 | tf_op args[6]
  146.9 8.9 %psum.39 = f32[2]{0:T(128)S(1)} all-reduce(f32[2]{0:T(128)S(1)} %psum.38), channel_id=1, replica_groups=mesh['fs'=4,'tp'=8] {'fs'}, use_global_device_ids=true, to_apply=%region_5.0 | all-reduce | flops 2 | bytes 16 | tf_op jit(solution)/shard_map/psum | solution.py:59
  155.8 3.1 %broadcast_multiply_fusion = f32[2,1024,512]{2,1,0:T(8,128)S(1)} fusion(f32[2,1024,512]{2,1,0:T(8,128)} %get-tuple-element.21, f32[2]{0:T(128)S(1)} %add_rsqrt_fusion), kind=kLoop, calls=%fused_computation.7 | loop fusion | flops 1048576 | bytes 8388616 | tf_op jit(solution)/shard_map/mul | solution.py:61
  158.9 2.6 fusion.15
  161.5 0.4 copy-done.1
  161.9 0.0 all-gather.3.cloned.1.call-start
  162.0 4.5 %fusion.17 = (bf16[1024,512]{1,0:T(8,128)(2,1)}, f32[1024,512]{1,0:T(8,128)}) fusion(f32[1024,512]{1,0:T(8,128)} %param.14, f32[2,1024,512]{2,1,0:T(8,128)} %copy-done.1), kind=kLoop, calls=%fused_computation.30 | loop fusion | flops 1572864 | bytes 7340032 | tf_op jit(solution)/shard_map/convert_element_type | solution.py:65
  166.5 3.1 %copy.16 = f32[512,1024]{1,0:T(8,128)} copy(f32[512,1024]{0,1:T(8,128)} %get-tuple-element.15) | data formatting | bytes 4194304
  169.5 42.3 %all-gather.5.cloned.1.call-done = bf16[512,4096]{0,1:T(8,128)(2,1)} async-done(((bf16[512,1024]{0,1:T(8,128)(2,1)}), bf16[512,4096]{0,1:T(8,128)(2,1)}) %all-gather.5.cloned.1.call-update) | async-done | bytes 4194320 | tf_op jit(solution)/shard_map/all_gather | solution.py:66
  211.9 6.3 %copy.17 = bf16[512,4096]{1,0:T(8,128)(2,1)} copy(bf16[512,4096]{0,1:T(8,128)(2,1)} %all-gather.5.cloned.1.call-done) | data formatting | bytes 8388608
  218.2 48.0 %all-gather.3.cloned.1.call-done = bf16[4096,512]{1,0:T(8,128)(2,1)} async-done(((bf16[1024,512]{1,0:T(8,128)(2,1)}), bf16[4096,512]{1,0:T(8,128)(2,1)}) %all-gather.3.cloned.1.call-update) | async-done | bytes 4194320 | tf_op jit(solution)/shard_map/all_gather | solution.py:65
  266.2 4.5 %copy.22 = bf16[4096,512]{1,0:T(8,128)(2,1)} copy(bf16[4096,512]{1,0:T(8,128)(2,1)} %all-gather.3.cloned.1.call-done) | data formatting | bytes 8388608
  (19 shorter events, 0.2 us)
Async XLA Ops:
  7.2 1.6 copy-start
  7.2 66.9 %copy-start.5 = (bf16[672,512]{1,0:T(8,128)(2,1)S(1)}, bf16[672,512]{1,0:T(8,128)(2,1)}, u32[]{:S(2)}) copy-start(bf16[672,512]{1,0:T(8,128)(2,1)} %param.11) | copy-start | bytes 2064388
  7.2 66.9 %all-reduce.6.cloned.1.call-start = ((), (), s32[]{:S(2)}) async-start(), calls=%async_computation.3 | async-start | bytes 1572864 | tf_op jit(solution)/shard_map/psum | solution.py:46
  8.8 66.8 %copy-start.6 = (bf16[672,512]{1,0:T(8,128)(2,1)S(1)}, bf16[672,512]{1,0:T(8,128)(2,1)}, u32[]{:S(2)}) copy-start(bf16[672,512]{1,0:T(8,128)(2,1)} %param.10) | copy-start | bytes 2064388
  13.3 109.3 %all-reduce.4.cloned.1.call-start = ((), (), s32[]{:S(2)}) async-start(), calls=%async_computation | async-start | bytes 1048576 | tf_op jit(solution)/shard_map/psum | solution.py:53
  77.9 133.9 %all-gather.5.cloned.1.call-start = ((), (), s32[]{:S(2)}) async-start(), calls=%async_computation.2 | async-start | bytes 5242880 | tf_op jit(solution)/shard_map/all_gather | solution.py:66
  124.2 4.0 %copy-start.3 = (f32[2,128,512]{2,1,0:T(8,128)}, f32[2,128,512]{2,1,0:T(8,128)S(1)}, u32[]{:S(2)}) copy-start(f32[2,128,512]{2,1,0:T(8,128)S(1)} %get-tuple-element.33) | copy-start | bytes 1572868
  124.2 4.0 %copy-start.4 = (f32[2,128,512]{2,1,0:T(8,128)}, f32[2,128,512]{2,1,0:T(8,128)S(1)}, u32[]{:S(2)}) copy-start(f32[2,128,512]{2,1,0:T(8,128)S(1)} %get-tuple-element.32) | copy-start | bytes 1572868
  155.8 3.1 %copy-start.2 = (f32[512,1024]{0,1:T(8,128)S(1)}, f32[512,1024]{0,1:T(8,128)}, u32[]{:S(2)}) copy-start(f32[512,1024]{0,1:T(8,128)} %copy.15) | copy-start | bytes 6291460
  158.9 3.0 %copy-start.1 = (f32[2,1024,512]{2,1,0:T(8,128)}, f32[2,1024,512]{2,1,0:T(8,128)S(1)}, u32[]{:S(2)}) copy-start(f32[2,1024,512]{2,1,0:T(8,128)S(1)} %broadcast_multiply_fusion) | copy-start | bytes 12582916
  161.9 104.3 %all-gather.3.cloned.1.call-start = ((), (), s32[]{:S(2)}) async-start(), calls=%async_computation.1 | async-start | bytes 5242880 | tf_op jit(solution)/shard_map/all_gather | solution.py:65
Sparse Core Ops, SparseCore 0:
  13.4 60.6 all-reduce.5
  78.1 44.4 all-reduce.3
  162.0 49.7 all-gather.4
  213.6 52.5 all-gather.2
